TPU v7x, 128 devices: a whole 4x4x4 slice. The times are simulated.
128 devices in a mesh: sp: 16 (over z, y), tp: 8 (over x, core).
Axes of the slice: x: 4, y: 4, z: 4, core: 2. Of those that a mesh axis runs over, the one named last changes fastest.
Arguments:
- residual_in: bfloat16 [16384, 2048], P(('sp', 'tp')), may hold values from -6 to 6
- queries: bfloat16 [16384, 2048], P('sp', 'tp'), may hold values from -6 to 6
- keys: bfloat16 [16384, 1024], P('sp', 'tp'), may hold values from -6 to 6
- values: bfloat16 [16384, 1024], P('sp', 'tp'), may hold values from -6 to 6
- query_gain: float32 [128], replicated, may hold values from 1 to 7
- key_norm_gain: float32 [128], replicated, may hold values from 1 to 7
- out_weight: bfloat16 [2048, 2048], replicated, may hold values from -0.125 to 0.125
- norm_gain: float32 [2048], replicated, may hold values from 0.1 to 1.9
- up_weight: bfloat16 [2048, 8192], P('sp', 'tp'), may hold values from -0.125 to 0.125
- down_weight: bfloat16 [8192, 2048], P('tp', 'sp'), may hold values from -0.0625 to 0.0625
Outputs:
- residual_out: bfloat16 [16384, 2048], P(('sp', 'tp'))
All inputs are finite; a program needn't handle non-finite values.
Results may differ from a plain program's by a relative error of at most 0.017.
The roundings to bfloat16 on the way count: a program that leaves them out, or rounds other values in their place, can miss the bound.
Values may be sent and summed in bfloat16 or wider, within the bound.
No kernel may reach another device: no remote copies, remote signals or barrier semaphores. Data moves between devices by JAX's collectives and lax.ppermute only.
A program may use at most 128 MiB of HBM per device.

v0:
```python
import jax
import jax.numpy as jnp
from jax import lax
from jax.sharding import PartitionSpec as P

HEAD_WIDTH = 128
GRID_W = 64
epsilon = 1e-06


def sent_together(arrays, axis, dim, along):
    widths = [a.shape[along] for a in arrays]
    both = jnp.concatenate(arrays, axis=along)
    filled = lax.all_gather(both, axis, axis=dim, tiled=True)
    return tuple(jnp.split(filled, [sum(widths[:k]) for k in range(1, len(widths))], axis=along))


def rope_tables(offset, count):
    places = offset + jnp.arange(count)
    grid_row = (places // GRID_W).astype(jnp.float32)
    grid_col = (places % GRID_W).astype(jnp.float32)
    quarter = HEAD_WIDTH // 4
    inverse = 10000.0 ** (-jnp.arange(quarter, dtype=jnp.float32) / quarter)
    angle_row = grid_row[:, None] * inverse
    angle_col = grid_col[:, None] * inverse
    angles = jnp.concatenate([angle_row, angle_row, angle_col, angle_col], axis=-1)
    return (jnp.cos(angles), jnp.sin(angles))


def normalize_rotate(source, gain, cosine_lookup, sine_lookup):
    count = source.shape[0]
    heads = source.shape[1] // HEAD_WIDTH
    quarter = HEAD_WIDTH // 4
    vector = source.astype(jnp.float32).reshape(count, heads, HEAD_WIDTH)
    vector = vector * lax.rsqrt(jnp.mean(vector * vector, axis=-1, keepdims=True) + epsilon) * gain
    turned = jnp.concatenate(
        [
            -vector[..., quarter : 2 * quarter],
            vector[..., :quarter],
            -vector[..., 3 * quarter :],
            vector[..., 2 * quarter : 3 * quarter],
        ],
        axis=-1,
    )
    rotated = vector * cosine_lookup[:, None, :] + turned * sine_lookup[:, None, :]
    return rotated.reshape(count, heads * HEAD_WIDTH).astype(jnp.bfloat16)


def attend(state_now, key_rows, value_rows, query_grid):
    best, mass, accum = state_now
    kv_here = query_grid.shape[1]
    key_lattice = key_rows.reshape(key_rows.shape[0], kv_here, HEAD_WIDTH)
    value_lattice = value_rows.reshape(value_rows.shape[0], kv_here, HEAD_WIDTH)
    scores = jnp.einsum(
        "tkgd,rkd->tkgr", query_grid, key_lattice, preferred_element_type=jnp.float32
    ) * HEAD_WIDTH ** (-0.5)
    newest = jnp.maximum(best, jnp.max(scores, axis=-1))
    factor = jnp.exp(best - newest)
    weights = jnp.exp(scores - newest[..., None])
    mass = mass * factor + jnp.sum(weights, axis=-1)
    accum = accum * factor[..., None] + jnp.einsum(
        "tkgr,rkd->tkgd",
        weights.astype(jnp.bfloat16),
        value_lattice,
        preferred_element_type=jnp.float32,
    )
    return (newest, mass, accum)


def local(
    residual_in,
    queries,
    keys,
    values,
    query_gain,
    key_norm_gain,
    out_weight,
    norm_gain,
    up_weight,
    down_weight,
):
    tok_rows = queries.shape[0]
    heads_here = queries.shape[1] // HEAD_WIDTH
    kv_here = keys.shape[1] // HEAD_WIDTH
    queries_per_group = heads_here // kv_here
    cosine_lookup, sine_lookup = rope_tables(lax.axis_index("sp") * tok_rows, tok_rows)
    query_normalize = normalize_rotate(queries, query_gain, cosine_lookup, sine_lookup)
    key_normalize = normalize_rotate(keys, key_norm_gain, cosine_lookup, sine_lookup)
    query_grid = query_normalize.reshape(tok_rows, kv_here, queries_per_group, HEAD_WIDTH)
    initial = (
        jnp.full((tok_rows, kv_here, queries_per_group), -1e30, jnp.float32),
        jnp.zeros((tok_rows, kv_here, queries_per_group), jnp.float32),
        jnp.zeros((tok_rows, kv_here, queries_per_group, HEAD_WIDTH), jnp.float32),
    )
    state_now = initial
    key_rows, value_rows = sent_together((key_normalize, values), "sp", 0, 1)
    row_count = key_rows.shape[0]
    key_blocks = key_rows.reshape(row_count // 1024, 1024, key_rows.shape[1])
    value_blocks = value_rows.reshape(row_count // 1024, 1024, value_rows.shape[1])

    def step_block(state_block, block_pair):
        return (attend(state_block, block_pair[0], block_pair[1], query_grid), None)

    state_now, unused = lax.scan(step_block, state_now, (key_blocks, value_blocks))
    best, mass, accum = state_now
    attn = (accum / mass[..., None]).astype(jnp.bfloat16).reshape(tok_rows, heads_here * HEAD_WIDTH)
    all_heads = lax.all_to_all(attn, "tp", split_axis=0, concat_axis=1, tiled=True)
    projected = jnp.dot(all_heads, out_weight, preferred_element_type=jnp.float32)
    middle = residual_in.astype(jnp.float32) + projected
    normed = (
        middle * lax.rsqrt(jnp.mean(middle * middle, axis=-1, keepdims=True) + epsilon) * norm_gain
    ).astype(jnp.bfloat16)
    whole_rows = lax.all_gather(normed, "tp", axis=0, tiled=True)
    hidden = jax.nn.relu(
        jnp.dot(
            whole_rows,
            lax.all_gather(up_weight, "sp", axis=0, tiled=True),
            preferred_element_type=jnp.float32,
        )
    )
    act = (hidden * hidden).astype(jnp.bfloat16)
    down_whole = lax.all_gather(down_weight, "sp", axis=1, tiled=True)
    down = lax.psum_scatter(
        jnp.dot(act, down_whole, preferred_element_type=jnp.float32).astype(jnp.bfloat16),
        "tp",
        scatter_dimension=0,
        tiled=True,
    ).astype(jnp.float32)
    return (middle + down).astype(jnp.bfloat16)


def solution(mesh):
    return jax.shard_map(
        local,
        mesh=mesh,
        in_specs=(
            P(("sp", "tp"), None),
            P("sp", "tp"),
            P("sp", "tp"),
            P("sp", "tp"),
            P(),
            P(),
            P(),
            P(),
            P("sp", "tp"),
            P("tp", "sp"),
        ),
        out_specs=P(("sp", "tp"), None),
        check_vma=False,
    )
```

profile of v0, /device:TPU:0, one launch (start us, length us, event | category | flops | bytes accessed | tf_op | source)
XLA Modules:
  0.0 411.6 jit_solution(3915185514579296366)
XLA Ops:
  22.2 67.3 %all-gather.5.cloned.1.call-done = bf16[16384,256]{1,0:T(8,128)(2,1)} async-done(((bf16[1024,256]{1,0:T(8,128)(2,1)}), bf16[16384,256]{1,0:T(8,128)(2,1)}) %all-gather.5.cloned.1.call-update) | async-done | bytes 8388624 | tf_op jit(solution)/shard_map/all_gather | solution.py:14
  89.5 5.7 %fusion.46 = (bf16[16384,128]{1,0:T(8,128)(2,1)}, bf16[16384,128]{1,0:T(8,128)(2,1)}) fusion(bf16[16384,256]{1,0:T(8,128)(2,1)} %all-gather.5.cloned.1.call-done), kind=kLoop, calls=%fused_computation.85 | loop fusion | bytes 16777216 | tf_op jit(solution)/shard_map/split | solution.py:15
  95.2 204.8 %while.15 = (s32[]{:T(128)}, f32[1024,1,2]{0,2,1:T(2,128)S(1)}, f32[1024,1,2]{0,2,1:T(2,128)S(1)}, f32[1024,1,2,128]{0,3,2,1:T(8,128)S(1)}, bf16[16,1024,128]{2,...) while((s32[]{:T(128)}, f32[1024,1,2]{0,2,1:T(2,128)S(1)}, ...), condition=%wide.region_5.6_spmd.clone, body=%wide.region_2.5_spmd.clone.sunk | while | flops 1091317760 | bytes 61998208 | solution.py:104
  100.6 5.6 %fusion.61 = f32[1024,1,2,128]{0,3,2,1:T(8,128)S(1)} fusion(f32[1024,1024,2]{1,0,2:T(8,128)} %get-tuple-element.178, f32[1024,2]{0,1:T(2,128)S(1)} %bitcast.126, f32[1024,1,2,128]{0,3,2,1:T(8,128)S(1)} %get-tuple-element.192, f32[1024,2]{0,1:T(2,128)S(1)} %get-tuple-element.179, pred[]{:T(512)S(6)} %compare.14, ...), kind=kOutput, calls=%fused_computation.10.clone.1 | convolution fusion | flops 543948800 | bytes 10764801 | tf_op jit(solution)/shard_map/while/body/eval_jaxpr/tkgr,rkd->tkgd/dot_general | solution.py:61
  108.0 5.4 %bitcast_reduce_fusion.2 = (f32[1024,2]{0,1:T(2,128)S(1)}, f32[1024,1024,2]{1,0,2:T(8,128)}) fusion(bf16[1024,1,2,128]{3,0,2,1:T(8,128)(2,1)S(1)} %get-tuple-element.203, bf16[16,1024,128]{2,1,0:T(8,128)(2,1)} %get-tuple-element.202, s32[]{:T(128)} %get-tuple-element.189), kind=kOutput, calls=%fused_computation.1.clone.1 | convolution fusion | flops 541063168 | bytes 9183744 | tf_op jit(solution)/shard_map/while/body/eval_jaxpr/tkgd,rkd->tkgr/dot_general | solution.py:54
  113.5 5.5 %fusion.61 = f32[1024,1,2,128]{0,3,2,1:T(8,128)S(1)} fusion(f32[1024,1024,2]{1,0,2:T(8,128)} %get-tuple-element.178, f32[1024,2]{0,1:T(2,128)S(1)} %bitcast.126, f32[1024,1,2,128]{0,3,2,1:T(8,128)S(1)} %get-tuple-element.192, f32[1024,2]{0,1:T(2,128)S(1)} %get-tuple-element.179, pred[]{:T(512)S(6)} %compare.14, ...), kind=kOutput, calls=%fused_computation.10.clone.1 | convolution fusion | flops 543948800 | bytes 10764801 | tf_op jit(solution)/shard_map/while/body/eval_jaxpr/tkgr,rkd->tkgd/dot_general | solution.py:61
  120.8 5.4 %bitcast_reduce_fusion.2 = (f32[1024,2]{0,1:T(2,128)S(1)}, f32[1024,1024,2]{1,0,2:T(8,128)}) fusion(bf16[1024,1,2,128]{3,0,2,1:T(8,128)(2,1)S(1)} %get-tuple-element.203, bf16[16,1024,128]{2,1,0:T(8,128)(2,1)} %get-tuple-element.202, s32[]{:T(128)} %get-tuple-element.189), kind=kOutput, calls=%fused_computation.1.clone.1 | convolution fusion | flops 541063168 | bytes 9183744 | tf_op jit(solution)/shard_map/while/body/eval_jaxpr/tkgd,rkd->tkgr/dot_general | solution.py:54
  126.2 5.5 %fusion.61 = f32[1024,1,2,128]{0,3,2,1:T(8,128)S(1)} fusion(f32[1024,1024,2]{1,0,2:T(8,128)} %get-tuple-element.178, f32[1024,2]{0,1:T(2,128)S(1)} %bitcast.126, f32[1024,1,2,128]{0,3,2,1:T(8,128)S(1)} %get-tuple-element.192, f32[1024,2]{0,1:T(2,128)S(1)} %get-tuple-element.179, pred[]{:T(512)S(6)} %compare.14, ...), kind=kOutput, calls=%fused_computation.10.clone.1 | convolution fusion | flops 543948800 | bytes 10764801 | tf_op jit(solution)/shard_map/while/body/eval_jaxpr/tkgr,rkd->tkgd/dot_general | solution.py:61
  133.5 5.4 %bitcast_reduce_fusion.2 = (f32[1024,2]{0,1:T(2,128)S(1)}, f32[1024,1024,2]{1,0,2:T(8,128)}) fusion(bf16[1024,1,2,128]{3,0,2,1:T(8,128)(2,1)S(1)} %get-tuple-element.203, bf16[16,1024,128]{2,1,0:T(8,128)(2,1)} %get-tuple-element.202, s32[]{:T(128)} %get-tuple-element.189), kind=kOutput, calls=%fused_computation.1.clone.1 | convolution fusion | flops 541063168 | bytes 9183744 | tf_op jit(solution)/shard_map/while/body/eval_jaxpr/tkgd,rkd->tkgr/dot_general | solution.py:54
  139.0 5.6 %fusion.61 = f32[1024,1,2,128]{0,3,2,1:T(8,128)S(1)} fusion(f32[1024,1024,2]{1,0,2:T(8,128)} %get-tuple-element.178, f32[1024,2]{0,1:T(2,128)S(1)} %bitcast.126, f32[1024,1,2,128]{0,3,2,1:T(8,128)S(1)} %get-tuple-element.192, f32[1024,2]{0,1:T(2,128)S(1)} %get-tuple-element.179, pred[]{:T(512)S(6)} %compare.14, ...), kind=kOutput, calls=%fused_computation.10.clone.1 | convolution fusion | flops 543948800 | bytes 10764801 | tf_op jit(solution)/shard_map/while/body/eval_jaxpr/tkgr,rkd->tkgd/dot_general | solution.py:61
  146.6 5.4 %bitcast_reduce_fusion.2 = (f32[1024,2]{0,1:T(2,128)S(1)}, f32[1024,1024,2]{1,0,2:T(8,128)}) fusion(bf16[1024,1,2,128]{3,0,2,1:T(8,128)(2,1)S(1)} %get-tuple-element.203, bf16[16,1024,128]{2,1,0:T(8,128)(2,1)} %get-tuple-element.202, s32[]{:T(128)} %get-tuple-element.189), kind=kOutput, calls=%fused_computation.1.clone.1 | convolution fusion | flops 541063168 | bytes 9183744 | tf_op jit(solution)/shard_map/while/body/eval_jaxpr/tkgd,rkd->tkgr/dot_general | solution.py:54
  152.0 5.5 %fusion.61 = f32[1024,1,2,128]{0,3,2,1:T(8,128)S(1)} fusion(f32[1024,1024,2]{1,0,2:T(8,128)} %get-tuple-element.178, f32[1024,2]{0,1:T(2,128)S(1)} %bitcast.126, f32[1024,1,2,128]{0,3,2,1:T(8,128)S(1)} %get-tuple-element.192, f32[1024,2]{0,1:T(2,128)S(1)} %get-tuple-element.179, pred[]{:T(512)S(6)} %compare.14, ...), kind=kOutput, calls=%fused_computation.10.clone.1 | convolution fusion | flops 543948800 | bytes 10764801 | tf_op jit(solution)/shard_map/while/body/eval_jaxpr/tkgr,rkd->tkgd/dot_general | solution.py:61
  159.3 5.4 %bitcast_reduce_fusion.2 = (f32[1024,2]{0,1:T(2,128)S(1)}, f32[1024,1024,2]{1,0,2:T(8,128)}) fusion(bf16[1024,1,2,128]{3,0,2,1:T(8,128)(2,1)S(1)} %get-tuple-element.203, bf16[16,1024,128]{2,1,0:T(8,128)(2,1)} %get-tuple-element.202, s32[]{:T(128)} %get-tuple-element.189), kind=kOutput, calls=%fused_computation.1.clone.1 | convolution fusion | flops 541063168 | bytes 9183744 | tf_op jit(solution)/shard_map/while/body/eval_jaxpr/tkgd,rkd->tkgr/dot_general | solution.py:54
  164.8 5.6 %fusion.61 = f32[1024,1,2,128]{0,3,2,1:T(8,128)S(1)} fusion(f32[1024,1024,2]{1,0,2:T(8,128)} %get-tuple-element.178, f32[1024,2]{0,1:T(2,128)S(1)} %bitcast.126, f32[1024,1,2,128]{0,3,2,1:T(8,128)S(1)} %get-tuple-element.192, f32[1024,2]{0,1:T(2,128)S(1)} %get-tuple-element.179, pred[]{:T(512)S(6)} %compare.14, ...), kind=kOutput, calls=%fused_computation.10.clone.1 | convolution fusion | flops 543948800 | bytes 10764801 | tf_op jit(solution)/shard_map/while/body/eval_jaxpr/tkgr,rkd->tkgd/dot_general | solution.py:61
  177.6 5.8 %fusion.61 = f32[1024,1,2,128]{0,3,2,1:T(8,128)S(1)} fusion(f32[1024,1024,2]{1,0,2:T(8,128)} %get-tuple-element.178, f32[1024,2]{0,1:T(2,128)S(1)} %bitcast.126, f32[1024,1,2,128]{0,3,2,1:T(8,128)S(1)} %get-tuple-element.192, f32[1024,2]{0,1:T(2,128)S(1)} %get-tuple-element.179, pred[]{:T(512)S(6)} %compare.14, ...), kind=kOutput, calls=%fused_computation.10.clone.1 | convolution fusion | flops 543948800 | bytes 10764801 | tf_op jit(solution)/shard_map/while/body/eval_jaxpr/tkgr,rkd->tkgd/dot_general | solution.py:61
  190.7 5.6 %fusion.61 = f32[1024,1,2,128]{0,3,2,1:T(8,128)S(1)} fusion(f32[1024,1024,2]{1,0,2:T(8,128)} %get-tuple-element.178, f32[1024,2]{0,1:T(2,128)S(1)} %bitcast.126, f32[1024,1,2,128]{0,3,2,1:T(8,128)S(1)} %get-tuple-element.192, f32[1024,2]{0,1:T(2,128)S(1)} %get-tuple-element.179, pred[]{:T(512)S(6)} %compare.14, ...), kind=kOutput, calls=%fused_computation.10.clone.1 | convolution fusion | flops 543948800 | bytes 10764801 | tf_op jit(solution)/shard_map/while/body/eval_jaxpr/tkgr,rkd->tkgd/dot_general | solution.py:61
  203.7 5.5 %fusion.61 = f32[1024,1,2,128]{0,3,2,1:T(8,128)S(1)} fusion(f32[1024,1024,2]{1,0,2:T(8,128)} %get-tuple-element.178, f32[1024,2]{0,1:T(2,128)S(1)} %bitcast.126, f32[1024,1,2,128]{0,3,2,1:T(8,128)S(1)} %get-tuple-element.192, f32[1024,2]{0,1:T(2,128)S(1)} %get-tuple-element.179, pred[]{:T(512)S(6)} %compare.14, ...), kind=kOutput, calls=%fused_computation.10.clone.1 | convolution fusion | flops 543948800 | bytes 10764801 | tf_op jit(solution)/shard_map/while/body/eval_jaxpr/tkgr,rkd->tkgd/dot_general | solution.py:61
  210.9 5.4 %bitcast_reduce_fusion.2 = (f32[1024,2]{0,1:T(2,128)S(1)}, f32[1024,1024,2]{1,0,2:T(8,128)}) fusion(bf16[1024,1,2,128]{3,0,2,1:T(8,128)(2,1)S(1)} %get-tuple-element.203, bf16[16,1024,128]{2,1,0:T(8,128)(2,1)} %get-tuple-element.202, s32[]{:T(128)} %get-tuple-element.189), kind=kOutput, calls=%fused_computation.1.clone.1 | convolution fusion | flops 541063168 | bytes 9183744 | tf_op jit(solution)/shard_map/while/body/eval_jaxpr/tkgd,rkd->tkgr/dot_general | solution.py:54
  216.4 5.5 %fusion.61 = f32[1024,1,2,128]{0,3,2,1:T(8,128)S(1)} fusion(f32[1024,1024,2]{1,0,2:T(8,128)} %get-tuple-element.178, f32[1024,2]{0,1:T(2,128)S(1)} %bitcast.126, f32[1024,1,2,128]{0,3,2,1:T(8,128)S(1)} %get-tuple-element.192, f32[1024,2]{0,1:T(2,128)S(1)} %get-tuple-element.179, pred[]{:T(512)S(6)} %compare.14, ...), kind=kOutput, calls=%fused_computation.10.clone.1 | convolution fusion | flops 543948800 | bytes 10764801 | tf_op jit(solution)/shard_map/while/body/eval_jaxpr/tkgr,rkd->tkgd/dot_general | solution.py:61
  223.7 5.4 %bitcast_reduce_fusion.2 = (f32[1024,2]{0,1:T(2,128)S(1)}, f32[1024,1024,2]{1,0,2:T(8,128)}) fusion(bf16[1024,1,2,128]{3,0,2,1:T(8,128)(2,1)S(1)} %get-tuple-element.203, bf16[16,1024,128]{2,1,0:T(8,128)(2,1)} %get-tuple-element.202, s32[]{:T(128)} %get-tuple-element.189), kind=kOutput, calls=%fused_computation.1.clone.1 | convolution fusion | flops 541063168 | bytes 9183744 | tf_op jit(solution)/shard_map/while/body/eval_jaxpr/tkgd,rkd->tkgr/dot_general | solution.py:54
  229.1 5.5 %fusion.61 = f32[1024,1,2,128]{0,3,2,1:T(8,128)S(1)} fusion(f32[1024,1024,2]{1,0,2:T(8,128)} %get-tuple-element.178, f32[1024,2]{0,1:T(2,128)S(1)} %bitcast.126, f32[1024,1,2,128]{0,3,2,1:T(8,128)S(1)} %get-tuple-element.192, f32[1024,2]{0,1:T(2,128)S(1)} %get-tuple-element.179, pred[]{:T(512)S(6)} %compare.14, ...), kind=kOutput, calls=%fused_computation.10.clone.1 | convolution fusion | flops 543948800 | bytes 10764801 | tf_op jit(solution)/shard_map/while/body/eval_jaxpr/tkgr,rkd->tkgd/dot_general | solution.py:61
  236.4 5.4 %bitcast_reduce_fusion.2 = (f32[1024,2]{0,1:T(2,128)S(1)}, f32[1024,1024,2]{1,0,2:T(8,128)}) fusion(bf16[1024,1,2,128]{3,0,2,1:T(8,128)(2,1)S(1)} %get-tuple-element.203, bf16[16,1024,128]{2,1,0:T(8,128)(2,1)} %get-tuple-element.202, s32[]{:T(128)} %get-tuple-element.189), kind=kOutput, calls=%fused_computation.1.clone.1 | convolution fusion | flops 541063168 | bytes 9183744 | tf_op jit(solution)/shard_map/while/body/eval_jaxpr/tkgd,rkd->tkgr/dot_general | solution.py:54
  241.8 5.5 %fusion.61 = f32[1024,1,2,128]{0,3,2,1:T(8,128)S(1)} fusion(f32[1024,1024,2]{1,0,2:T(8,128)} %get-tuple-element.178, f32[1024,2]{0,1:T(2,128)S(1)} %bitcast.126, f32[1024,1,2,128]{0,3,2,1:T(8,128)S(1)} %get-tuple-element.192, f32[1024,2]{0,1:T(2,128)S(1)} %get-tuple-element.179, pred[]{:T(512)S(6)} %compare.14, ...), kind=kOutput, calls=%fused_computation.10.clone.1 | convolution fusion | flops 543948800 | bytes 10764801 | tf_op jit(solution)/shard_map/while/body/eval_jaxpr/tkgr,rkd->tkgd/dot_general | solution.py:61
  249.1 5.4 %bitcast_reduce_fusion.2 = (f32[1024,2]{0,1:T(2,128)S(1)}, f32[1024,1024,2]{1,0,2:T(8,128)}) fusion(bf16[1024,1,2,128]{3,0,2,1:T(8,128)(2,1)S(1)} %get-tuple-element.203, bf16[16,1024,128]{2,1,0:T(8,128)(2,1)} %get-tuple-element.202, s32[]{:T(128)} %get-tuple-element.189), kind=kOutput, calls=%fused_computation.1.clone.1 | convolution fusion | flops 541063168 | bytes 9183744 | tf_op jit(solution)/shard_map/while/body/eval_jaxpr/tkgd,rkd->tkgr/dot_general | solution.py:54
  254.6 5.5 %fusion.61 = f32[1024,1,2,128]{0,3,2,1:T(8,128)S(1)} fusion(f32[1024,1024,2]{1,0,2:T(8,128)} %get-tuple-element.178, f32[1024,2]{0,1:T(2,128)S(1)} %bitcast.126, f32[1024,1,2,128]{0,3,2,1:T(8,128)S(1)} %get-tuple-element.192, f32[1024,2]{0,1:T(2,128)S(1)} %get-tuple-element.179, pred[]{:T(512)S(6)} %compare.14, ...), kind=kOutput, calls=%fused_computation.10.clone.1 | convolution fusion | flops 543948800 | bytes 10764801 | tf_op jit(solution)/shard_map/while/body/eval_jaxpr/tkgr,rkd->tkgd/dot_general | solution.py:61
  267.3 5.5 %fusion.61 = f32[1024,1,2,128]{0,3,2,1:T(8,128)S(1)} fusion(f32[1024,1024,2]{1,0,2:T(8,128)} %get-tuple-element.178, f32[1024,2]{0,1:T(2,128)S(1)} %bitcast.126, f32[1024,1,2,128]{0,3,2,1:T(8,128)S(1)} %get-tuple-element.192, f32[1024,2]{0,1:T(2,128)S(1)} %get-tuple-element.179, pred[]{:T(512)S(6)} %compare.14, ...), kind=kOutput, calls=%fused_computation.10.clone.1 | convolution fusion | flops 543948800 | bytes 10764801 | tf_op jit(solution)/shard_map/while/body/eval_jaxpr/tkgr,rkd->tkgd/dot_general | solution.py:61
  280.0 5.5 %fusion.61 = f32[1024,1,2,128]{0,3,2,1:T(8,128)S(1)} fusion(f32[1024,1024,2]{1,0,2:T(8,128)} %get-tuple-element.178, f32[1024,2]{0,1:T(2,128)S(1)} %bitcast.126, f32[1024,1,2,128]{0,3,2,1:T(8,128)S(1)} %get-tuple-element.192, f32[1024,2]{0,1:T(2,128)S(1)} %get-tuple-element.179, pred[]{:T(512)S(6)} %compare.14, ...), kind=kOutput, calls=%fused_computation.10.clone.1 | convolution fusion | flops 543948800 | bytes 10764801 | tf_op jit(solution)/shard_map/while/body/eval_jaxpr/tkgr,rkd->tkgd/dot_general | solution.py:61
  292.7 5.5 %fusion.61 = f32[1024,1,2,128]{0,3,2,1:T(8,128)S(1)} fusion(f32[1024,1024,2]{1,0,2:T(8,128)} %get-tuple-element.178, f32[1024,2]{0,1:T(2,128)S(1)} %bitcast.126, f32[1024,1,2,128]{0,3,2,1:T(8,128)S(1)} %get-tuple-element.192, f32[1024,2]{0,1:T(2,128)S(1)} %get-tuple-element.179, pred[]{:T(512)S(6)} %compare.14, ...), kind=kOutput, calls=%fused_computation.10.clone.1 | convolution fusion | flops 543948800 | bytes 10764801 | tf_op jit(solution)/shard_map/while/body/eval_jaxpr/tkgr,rkd->tkgd/dot_general | solution.py:61
  300.3 14.4 %all_to_all.19 = bf16[8,128,256]{1,2,0:T(8,128)(2,1)S(1)} all-to-all(bf16[8,128,256]{1,2,0:T(8,128)(2,1)S(1)} %copy.31), channel_id=1, replica_groups=mesh['sp'=16,'tp'=8] {'tp'}, dimensions={0} | all-to-all | bytes 1048576 | tf_op jit(solution)/shard_map/all_to_all | solution.py:107
  320.8 29.9 %all-gather.7.cloned.1.call-done = bf16[1024,2048]{1,0:T(8,128)(2,1)} async-done(((bf16[128,2048]{1,0:T(8,128)(2,1)}), bf16[1024,2048]{1,0:T(8,128)(2,1)}) %all-gather.7.cloned.1.call-update) | async-done | bytes 4194320 | tf_op jit(solution)/shard_map/all_gather | solution.py:113
  350.7 14.4 %convolution_convert_fusion = bf16[1024,2048]{1,0:T(8,128)(2,1)} fusion(bf16[1024,2048]{1,0:T(8,128)(2,1)} %all-gather.11.cloned.1.call-done, bf16[1024,2048]{1,0:T(8,128)(2,1)} %all-gather.7.cloned.1.call-done, bf16[2048,1024]{1,0:T(8,128)(2,1)} %all-gather.9.cloned.1.call-done), kind=kOutput, calls=%fused_computation.28 | convolution fusion | flops 8595177472 | bytes 16777216 | tf_op jit(solution)/shard_map/dot_general | solution.py:124
  365.1 38.0 %reduce-scatter.2.cloned.1.call-done = bf16[128,2048]{1,0:T(8,128)(2,1)} async-done(((bf16[1024,2048]{1,0:T(8,128)(2,1)}), bf16[128,2048]{1,0:T(8,128)(2,1)}) %reduce-scatter.2.cloned.1.call-update) | async-done | bytes 524304 | tf_op jit(solution)/shard_map/reduce_scatter | solution.py:123
  (157 shorter events, 90.6 us)
Async XLA Ops:
  6.5 4.4 %copy-start.1 = (bf16[1024,128]{1,0:T(8,128)(2,1)S(1)}, bf16[1024,128]{1,0:T(8,128)(2,1)}, u32[]{:S(2)}) copy-start(bf16[1024,128]{1,0:T(8,128)(2,1)} %param.14) | copy-start | bytes 786436
  6.5 4.4 %copy-start.5 = (f32[128]{0:T(128)S(1)}, f32[128]{0:T(128)}, u32[]{:S(2)}) copy-start(f32[128]{0:T(128)} %param.17) | copy-start | bytes 1540
  6.5 82.9 %all-gather.5.cloned.1.call-start = ((), (), s32[]{:S(2)}) async-start(), calls=%async_computation.2 | async-start | bytes 8912896 | tf_op jit(solution)/shard_map/all_gather | solution.py:14
  8.9 6.1 %copy-start.3 = (bf16[1024,128]{1,0:T(8,128)(2,1)S(1)}, bf16[1024,128]{1,0:T(8,128)(2,1)}, u32[]{:S(2)}) copy-start(bf16[1024,128]{1,0:T(8,128)(2,1)} %param.15) | copy-start | bytes 786436
  10.9 8.2 %copy-start.6 = (f32[128]{0:T(128)S(1)}, f32[128]{0:T(128)}, u32[]{:S(2)}) copy-start(f32[128]{0:T(128)} %param.16) | copy-start | bytes 1540
  15.9 304.9 %all-gather.11.cloned.1.call-start = ((), (), s32[]{:S(2)}) async-start(), calls=%async_computation.5 | async-start | bytes 4456448 | tf_op jit(solution)/shard_map/all_gather | solution.py:122
  16.6 304.2 %all-gather.9.cloned.1.call-start = ((), (), s32[]{:S(2)}) async-start(), calls=%async_computation.4 | async-start | bytes 4456448 | tf_op jit(solution)/shard_map/all_gather | solution.py:117
  17.4 333.3 %all-gather.7.cloned.1.call-start = ((), (), s32[]{:S(2)}) async-start(), calls=%async_computation.3 | async-start | bytes 4718592 | tf_op jit(solution)/shard_map/all_gather | solution.py:113
  100.6 6.0 %copy-start = (f32[1024,1024,2]{1,0,2:T(8,128)S(1)}, f32[1024,1024,2]{1,0,2:T(8,128)}, u32[]{:S(2)}) copy-start(f32[1024,1024,2]{1,0,2:T(8,128)} %get-tuple-element.178) | copy-start | bytes 25165828 | tf_op jit(solution)/shard_map/while
  113.5 5.8 %copy-start = (f32[1024,1024,2]{1,0,2:T(8,128)S(1)}, f32[1024,1024,2]{1,0,2:T(8,128)}, u32[]{:S(2)}) copy-start(f32[1024,1024,2]{1,0,2:T(8,128)} %get-tuple-element.178) | copy-start | bytes 25165828 | tf_op jit(solution)/shard_map/while
  126.2 5.8 %copy-start = (f32[1024,1024,2]{1,0,2:T(8,128)S(1)}, f32[1024,1024,2]{1,0,2:T(8,128)}, u32[]{:S(2)}) copy-start(f32[1024,1024,2]{1,0,2:T(8,128)} %get-tuple-element.178) | copy-start | bytes 25165828 | tf_op jit(solution)/shard_map/while
  138.9 6.2 %copy-start = (f32[1024,1024,2]{1,0,2:T(8,128)S(1)}, f32[1024,1024,2]{1,0,2:T(8,128)}, u32[]{:S(2)}) copy-start(f32[1024,1024,2]{1,0,2:T(8,128)} %get-tuple-element.178) | copy-start | bytes 25165828 | tf_op jit(solution)/shard_map/while
  152.0 5.8 %copy-start = (f32[1024,1024,2]{1,0,2:T(8,128)S(1)}, f32[1024,1024,2]{1,0,2:T(8,128)}, u32[]{:S(2)}) copy-start(f32[1024,1024,2]{1,0,2:T(8,128)} %get-tuple-element.178) | copy-start | bytes 25165828 | tf_op jit(solution)/shard_map/while
  164.7 6.0 %copy-start = (f32[1024,1024,2]{1,0,2:T(8,128)S(1)}, f32[1024,1024,2]{1,0,2:T(8,128)}, u32[]{:S(2)}) copy-start(f32[1024,1024,2]{1,0,2:T(8,128)} %get-tuple-element.178) | copy-start | bytes 25165828 | tf_op jit(solution)/shard_map/while
  177.6 6.2 %copy-start = (f32[1024,1024,2]{1,0,2:T(8,128)S(1)}, f32[1024,1024,2]{1,0,2:T(8,128)}, u32[]{:S(2)}) copy-start(f32[1024,1024,2]{1,0,2:T(8,128)} %get-tuple-element.178) | copy-start | bytes 25165828 | tf_op jit(solution)/shard_map/while
  190.6 6.1 %copy-start = (f32[1024,1024,2]{1,0,2:T(8,128)S(1)}, f32[1024,1024,2]{1,0,2:T(8,128)}, u32[]{:S(2)}) copy-start(f32[1024,1024,2]{1,0,2:T(8,128)} %get-tuple-element.178) | copy-start | bytes 25165828 | tf_op jit(solution)/shard_map/while
  203.7 5.8 %copy-start = (f32[1024,1024,2]{1,0,2:T(8,128)S(1)}, f32[1024,1024,2]{1,0,2:T(8,128)}, u32[]{:S(2)}) copy-start(f32[1024,1024,2]{1,0,2:T(8,128)} %get-tuple-element.178) | copy-start | bytes 25165828 | tf_op jit(solution)/shard_map/while
  216.4 5.8 %copy-start = (f32[1024,1024,2]{1,0,2:T(8,128)S(1)}, f32[1024,1024,2]{1,0,2:T(8,128)}, u32[]{:S(2)}) copy-start(f32[1024,1024,2]{1,0,2:T(8,128)} %get-tuple-element.178) | copy-start | bytes 25165828 | tf_op jit(solution)/shard_map/while
  229.1 5.8 %copy-start = (f32[1024,1024,2]{1,0,2:T(8,128)S(1)}, f32[1024,1024,2]{1,0,2:T(8,128)}, u32[]{:S(2)}) copy-start(f32[1024,1024,2]{1,0,2:T(8,128)} %get-tuple-element.178) | copy-start | bytes 25165828 | tf_op jit(solution)/shard_map/while
  241.8 5.8 %copy-start = (f32[1024,1024,2]{1,0,2:T(8,128)S(1)}, f32[1024,1024,2]{1,0,2:T(8,128)}, u32[]{:S(2)}) copy-start(f32[1024,1024,2]{1,0,2:T(8,128)} %get-tuple-element.178) | copy-start | bytes 25165828 | tf_op jit(solution)/shard_map/while
  254.6 5.8 %copy-start = (f32[1024,1024,2]{1,0,2:T(8,128)S(1)}, f32[1024,1024,2]{1,0,2:T(8,128)}, u32[]{:S(2)}) copy-start(f32[1024,1024,2]{1,0,2:T(8,128)} %get-tuple-element.178) | copy-start | bytes 25165828 | tf_op jit(solution)/shard_map/while
  267.3 5.8 %copy-start = (f32[1024,1024,2]{1,0,2:T(8,128)S(1)}, f32[1024,1024,2]{1,0,2:T(8,128)}, u32[]{:S(2)}) copy-start(f32[1024,1024,2]{1,0,2:T(8,128)} %get-tuple-element.178) | copy-start | bytes 25165828 | tf_op jit(solution)/shard_map/while
  280.0 5.8 %copy-start = (f32[1024,1024,2]{1,0,2:T(8,128)S(1)}, f32[1024,1024,2]{1,0,2:T(8,128)}, u32[]{:S(2)}) copy-start(f32[1024,1024,2]{1,0,2:T(8,128)} %get-tuple-element.178) | copy-start | bytes 25165828 | tf_op jit(solution)/shard_map/while
  292.7 5.8 %copy-start = (f32[1024,1024,2]{1,0,2:T(8,128)S(1)}, f32[1024,1024,2]{1,0,2:T(8,128)}, u32[]{:S(2)}) copy-start(f32[1024,1024,2]{1,0,2:T(8,128)} %get-tuple-element.178) | copy-start | bytes 25165828 | tf_op jit(solution)/shard_map/while
  300.0 14.7 %copy-start.2 = (bf16[128,2048]{1,0:T(8,128)(2,1)S(1)}, bf16[128,2048]{1,0:T(8,128)(2,1)}, u32[]{:S(2)}) copy-start(bf16[128,2048]{1,0:T(8,128)(2,1)} %param.12) | copy-start | bytes 1572868
  314.7 4.8 %copy-start.4 = (f32[2048]{0:T(1024)S(1)}, f32[2048]{0:T(1024)}, u32[]{:S(2)}) copy-start(f32[2048]{0:T(1024)} %param.19) | copy-start | bytes 24580
  320.5 82.6 %reduce-scatter.2.cloned.1.call-start = ((), (), s32[]{:S(2)}) async-start(), calls=%async_computation.6 | async-start | bytes 4718592 | tf_op jit(solution)/shard_map/reduce_scatter | solution.py:123
Sparse Core Ops, SparseCore 0:
  16.0 73.4 all-gather.4
  91.6 56.5 all-gather.10
  150.3 50.7 all-gather.8
  320.6 29.9 all-gather.6
  365.2 37.8 reduce-scatter.1
where the time goes:
time: 412 us
  matrix products  194 us (47%)
  waiting for transfers between devices  137 us (33%)
  other arithmetic  37.7 us (9%)
  blocking collectives  14.4 us (3%)
  local copies, waits for them, and re-layouts  14.1 us (3%)
  between operations  13.4 us (3%)
    dot_general x16, matrix products, attend(): jnp.einsum('tkgr,rkd->tkgd', weights.astype(jnp.bfloat16), value_lattice,...  88.3 us
    dot_general x16, matrix products, attend(): jnp.einsum('tkgd,rkd->tkgr', query_grid, key_lattice, preferred_element_t...  86.8 us
    all_gather x1, waiting for transfers between devices, sent_together(): filled = lax.all_gather(both, axis, axis=dim, tiled=True)  67.3 us
    reduce_scatter x1, waiting for transfers between devices, local(): lax.psum_scatter(jnp.dot(act, down_whole, preferred_element_type=jnp.floa...  38 us
    all_gather x1, waiting for transfers between devices, local(): whole_rows = lax.all_gather(normed, 'tp', axis=0, tiled=True)  29.9 us
    reduce_sum x16, other arithmetic, attend(): mass = mass * factor + jnp.sum(weights, axis=-1)  22.1 us
    all_to_all x1, blocking collectives, local(): lax.all_to_all(attn, 'tp', split_axis=0, concat_axis=1, tiled=True)  14.4 us
    dot_general x1, matrix products, local(): jnp.dot(act, down_whole, preferred_element_type=jnp.float32)  14.4 us
  transfers between devices with their start and end apart: 5, of which 3 were waited for; matrix products, arithmetic and copies ran while one was open for 52% of the time, Pallas kernels for 0%

commit v1 on v0

--- a/solution.py
+++ b/solution.py
@@ -110,7 +110,9 @@
     normed = (
         middle * lax.rsqrt(jnp.mean(middle * middle, axis=-1, keepdims=True) + epsilon) * norm_gain
     ).astype(jnp.bfloat16)
-    whole_rows = lax.all_gather(normed, "tp", axis=0, tiled=True)
+    whole_rows = jnp.concatenate(
+        lax.all_to_all(jnp.stack([normed] * lax.axis_size("tp")), "tp", 0, 0), axis=0
+    )
     hidden = jax.nn.relu(
         jnp.dot(
             whole_rows,

time: 412 us -> 436 us (1.058)
  waiting for transfers between devices: 137 us -> 154 us
  starting transfers between devices: 0.34 us -> 4.85 us
    all_to_all x0 -> x1, waiting for transfers between devices: none -> 49.4 us  [local(): lax.all_to_all(jnp.stack([normed] * lax.axis_size('tp')), 'tp', 0, 0)]
    all_gather x1 -> x0, waiting for transfers between devices: 29.9 us -> none  [local(): whole_rows = lax.all_gather(normed, 'tp', axis=0, tiled=True)]
    all_to_all x0 -> x1, starting transfers between devices: none -> 4.55 us  [local(): lax.all_to_all(jnp.stack([normed] * lax.axis_size('tp')), 'tp', 0, 0)]
  transfers between devices with their start and end apart: 5 -> 5, of which waited for: 3 -> 3; matrix products, arithmetic and copies ran while one was open for 52% -> 50% of each run, Pallas kernels for 0% -> 0%
where the time goes in v1:
time: 436 us; the launch traced here: 435 us
  matrix products  194 us (44%)
  waiting for transfers between devices  154 us (35%)
  other arithmetic  36.9 us (8%)
  local copies, waits for them, and re-layouts  16.7 us (4%)
  blocking collectives  14.4 us (3%)
  between operations  13.4 us (3%)
  starting transfers between devices  4.85 us (1%)
    dot_general x16, matrix products, attend(): jnp.einsum('tkgr,rkd->tkgd', weights.astype(jnp.bfloat16), value_lattice,...  88 us
    dot_general x16, matrix products, attend(): jnp.einsum('tkgd,rkd->tkgr', query_grid, key_lattice, preferred_element_t...  86.9 us
    all_gather x1, waiting for transfers between devices, sent_together(): filled = lax.all_gather(both, axis, axis=dim, tiled=True)  67.3 us
    all_to_all x1, waiting for transfers between devices, local(): lax.all_to_all(jnp.stack([normed] * lax.axis_size('tp')), 'tp', 0, 0)  49.4 us
    reduce_scatter x1, waiting for transfers between devices, local(): lax.psum_scatter(jnp.dot(act, down_whole, preferred_element_type=jnp.floa...  36.3 us
    reduce_sum x16, other arithmetic, attend(): mass = mass * factor + jnp.sum(weights, axis=-1)  22.1 us
    all_to_all x1, blocking collectives, local(): lax.all_to_all(attn, 'tp', split_axis=0, concat_axis=1, tiled=True)  14.4 us
    dot_general x1, matrix products, local(): jnp.dot(act, down_whole, preferred_element_type=jnp.float32)  14.4 us
  transfers between devices with their start and end apart: 5, of which 3 were waited for; matrix products, arithmetic and copies ran while one was open for 50% of the time, Pallas kernels for 0%

profile of v1, /device:TPU:0, one launch (start us, length us, event | category | flops | bytes accessed | tf_op | source)
XLA Modules:
  0.0 435.4 jit_solution(7121753132566006017)
XLA Ops:
  22.1 67.3 %all-gather.4.cloned.1.call-done = bf16[16384,256]{1,0:T(8,128)(2,1)} async-done(((bf16[1024,256]{1,0:T(8,128)(2,1)}), bf16[16384,256]{1,0:T(8,128)(2,1)}) %all-gather.4.cloned.1.call-update) | async-done | bytes 8388624 | tf_op jit(solution)/shard_map/all_gather | solution.py:14
  89.5 5.7 %fusion.46 = (bf16[16384,128]{1,0:T(8,128)(2,1)}, bf16[16384,128]{1,0:T(8,128)(2,1)}) fusion(bf16[16384,256]{1,0:T(8,128)(2,1)} %all-gather.4.cloned.1.call-done), kind=kLoop, calls=%fused_computation.85 | loop fusion | bytes 16777216 | tf_op jit(solution)/shard_map/split | solution.py:15
  95.2 204.7 %while.15 = (s32[]{:T(128)}, f32[1024,1,2]{0,2,1:T(2,128)S(1)}, f32[1024,1,2]{0,2,1:T(2,128)S(1)}, f32[1024,1,2,128]{0,3,2,1:T(8,128)S(1)}, bf16[16,1024,128]{2,...) while((s32[]{:T(128)}, f32[1024,1,2]{0,2,1:T(2,128)S(1)}, ...), condition=%wide.region_5.6_spmd.clone, body=%wide.region_2.5_spmd.clone.sunk | while | flops 1091317760 | bytes 61998208 | solution.py:104
  100.6 5.6 %fusion.61 = f32[1024,1,2,128]{0,3,2,1:T(8,128)S(1)} fusion(f32[1024,1024,2]{1,0,2:T(8,128)} %get-tuple-element.178, f32[1024,2]{0,1:T(2,128)S(1)} %bitcast.127, f32[1024,1,2,128]{0,3,2,1:T(8,128)S(1)} %get-tuple-element.192, f32[1024,2]{0,1:T(2,128)S(1)} %get-tuple-element.179, pred[]{:T(512)S(6)} %compare.14, ...), kind=kOutput, calls=%fused_computation.10.clone.1 | convolution fusion | flops 543948800 | bytes 10764801 | tf_op jit(solution)/shard_map/while/body/eval_jaxpr/tkgr,rkd->tkgd/dot_general | solution.py:61
  108.1 5.4 %bitcast_reduce_fusion.2 = (f32[1024,2]{0,1:T(2,128)S(1)}, f32[1024,1024,2]{1,0,2:T(8,128)}) fusion(bf16[1024,1,2,128]{3,0,2,1:T(8,128)(2,1)S(1)} %get-tuple-element.203, bf16[16,1024,128]{2,1,0:T(8,128)(2,1)} %get-tuple-element.202, s32[]{:T(128)} %get-tuple-element.189), kind=kOutput, calls=%fused_computation.1.clone.1 | convolution fusion | flops 541063168 | bytes 9183744 | tf_op jit(solution)/shard_map/while/body/eval_jaxpr/tkgd,rkd->tkgr/dot_general | solution.py:54
  113.5 5.5 %fusion.61 = f32[1024,1,2,128]{0,3,2,1:T(8,128)S(1)} fusion(f32[1024,1024,2]{1,0,2:T(8,128)} %get-tuple-element.178, f32[1024,2]{0,1:T(2,128)S(1)} %bitcast.127, f32[1024,1,2,128]{0,3,2,1:T(8,128)S(1)} %get-tuple-element.192, f32[1024,2]{0,1:T(2,128)S(1)} %get-tuple-element.179, pred[]{:T(512)S(6)} %compare.14, ...), kind=kOutput, calls=%fused_computation.10.clone.1 | convolution fusion | flops 543948800 | bytes 10764801 | tf_op jit(solution)/shard_map/while/body/eval_jaxpr/tkgr,rkd->tkgd/dot_general | solution.py:61
  120.8 5.4 %bitcast_reduce_fusion.2 = (f32[1024,2]{0,1:T(2,128)S(1)}, f32[1024,1024,2]{1,0,2:T(8,128)}) fusion(bf16[1024,1,2,128]{3,0,2,1:T(8,128)(2,1)S(1)} %get-tuple-element.203, bf16[16,1024,128]{2,1,0:T(8,128)(2,1)} %get-tuple-element.202, s32[]{:T(128)} %get-tuple-element.189), kind=kOutput, calls=%fused_computation.1.clone.1 | convolution fusion | flops 541063168 | bytes 9183744 | tf_op jit(solution)/shard_map/while/body/eval_jaxpr/tkgd,rkd->tkgr/dot_general | solution.py:54
  126.2 5.6 %fusion.61 = f32[1024,1,2,128]{0,3,2,1:T(8,128)S(1)} fusion(f32[1024,1024,2]{1,0,2:T(8,128)} %get-tuple-element.178, f32[1024,2]{0,1:T(2,128)S(1)} %bitcast.127, f32[1024,1,2,128]{0,3,2,1:T(8,128)S(1)} %get-tuple-element.192, f32[1024,2]{0,1:T(2,128)S(1)} %get-tuple-element.179, pred[]{:T(512)S(6)} %compare.14, ...), kind=kOutput, calls=%fused_computation.10.clone.1 | convolution fusion | flops 543948800 | bytes 10764801 | tf_op jit(solution)/shard_map/while/body/eval_jaxpr/tkgr,rkd->tkgd/dot_general | solution.py:61
  133.8 5.4 %bitcast_reduce_fusion.2 = (f32[1024,2]{0,1:T(2,128)S(1)}, f32[1024,1024,2]{1,0,2:T(8,128)}) fusion(bf16[1024,1,2,128]{3,0,2,1:T(8,128)(2,1)S(1)} %get-tuple-element.203, bf16[16,1024,128]{2,1,0:T(8,128)(2,1)} %get-tuple-element.202, s32[]{:T(128)} %get-tuple-element.189), kind=kOutput, calls=%fused_computation.1.clone.1 | convolution fusion | flops 541063168 | bytes 9183744 | tf_op jit(solution)/shard_map/while/body/eval_jaxpr/tkgd,rkd->tkgr/dot_general | solution.py:54
  139.2 5.5 %fusion.61 = f32[1024,1,2,128]{0,3,2,1:T(8,128)S(1)} fusion(f32[1024,1024,2]{1,0,2:T(8,128)} %get-tuple-element.178, f32[1024,2]{0,1:T(2,128)S(1)} %bitcast.127, f32[1024,1,2,128]{0,3,2,1:T(8,128)S(1)} %get-tuple-element.192, f32[1024,2]{0,1:T(2,128)S(1)} %get-tuple-element.179, pred[]{:T(512)S(6)} %compare.14, ...), kind=kOutput, calls=%fused_computation.10.clone.1 | convolution fusion | flops 543948800 | bytes 10764801 | tf_op jit(solution)/shard_map/while/body/eval_jaxpr/tkgr,rkd->tkgd/dot_general | solution.py:61
  146.5 5.4 %bitcast_reduce_fusion.2 = (f32[1024,2]{0,1:T(2,128)S(1)}, f32[1024,1024,2]{1,0,2:T(8,128)}) fusion(bf16[1024,1,2,128]{3,0,2,1:T(8,128)(2,1)S(1)} %get-tuple-element.203, bf16[16,1024,128]{2,1,0:T(8,128)(2,1)} %get-tuple-element.202, s32[]{:T(128)} %get-tuple-element.189), kind=kOutput, calls=%fused_computation.1.clone.1 | convolution fusion | flops 541063168 | bytes 9183744 | tf_op jit(solution)/shard_map/while/body/eval_jaxpr/tkgd,rkd->tkgr/dot_general | solution.py:54
  152.0 5.7 %fusion.61 = f32[1024,1,2,128]{0,3,2,1:T(8,128)S(1)} fusion(f32[1024,1024,2]{1,0,2:T(8,128)} %get-tuple-element.178, f32[1024,2]{0,1:T(2,128)S(1)} %bitcast.127, f32[1024,1,2,128]{0,3,2,1:T(8,128)S(1)} %get-tuple-element.192, f32[1024,2]{0,1:T(2,128)S(1)} %get-tuple-element.179, pred[]{:T(512)S(6)} %compare.14, ...), kind=kOutput, calls=%fused_computation.10.clone.1 | convolution fusion | flops 543948800 | bytes 10764801 | tf_op jit(solution)/shard_map/while/body/eval_jaxpr/tkgr,rkd->tkgd/dot_general | solution.py:61
  165.0 5.5 %fusion.61 = f32[1024,1,2,128]{0,3,2,1:T(8,128)S(1)} fusion(f32[1024,1024,2]{1,0,2:T(8,128)} %get-tuple-element.178, f32[1024,2]{0,1:T(2,128)S(1)} %bitcast.127, f32[1024,1,2,128]{0,3,2,1:T(8,128)S(1)} %get-tuple-element.192, f32[1024,2]{0,1:T(2,128)S(1)} %get-tuple-element.179, pred[]{:T(512)S(6)} %compare.14, ...), kind=kOutput, calls=%fused_computation.10.clone.1 | convolution fusion | flops 543948800 | bytes 10764801 | tf_op jit(solution)/shard_map/while/body/eval_jaxpr/tkgr,rkd->tkgd/dot_general | solution.py:61
  177.8 5.5 %fusion.61 = f32[1024,1,2,128]{0,3,2,1:T(8,128)S(1)} fusion(f32[1024,1024,2]{1,0,2:T(8,128)} %get-tuple-element.178, f32[1024,2]{0,1:T(2,128)S(1)} %bitcast.127, f32[1024,1,2,128]{0,3,2,1:T(8,128)S(1)} %get-tuple-element.192, f32[1024,2]{0,1:T(2,128)S(1)} %get-tuple-element.179, pred[]{:T(512)S(6)} %compare.14, ...), kind=kOutput, calls=%fused_computation.10.clone.1 | convolution fusion | flops 543948800 | bytes 10764801 | tf_op jit(solution)/shard_map/while/body/eval_jaxpr/tkgr,rkd->tkgd/dot_general | solution.py:61
  190.5 5.5 %fusion.61 = f32[1024,1,2,128]{0,3,2,1:T(8,128)S(1)} fusion(f32[1024,1024,2]{1,0,2:T(8,128)} %get-tuple-element.178, f32[1024,2]{0,1:T(2,128)S(1)} %bitcast.127, f32[1024,1,2,128]{0,3,2,1:T(8,128)S(1)} %get-tuple-element.192, f32[1024,2]{0,1:T(2,128)S(1)} %get-tuple-element.179, pred[]{:T(512)S(6)} %compare.14, ...), kind=kOutput, calls=%fused_computation.10.clone.1 | convolution fusion | flops 543948800 | bytes 10764801 | tf_op jit(solution)/shard_map/while/body/eval_jaxpr/tkgr,rkd->tkgd/dot_general | solution.py:61
  203.5 5.5 %fusion.61 = f32[1024,1,2,128]{0,3,2,1:T(8,128)S(1)} fusion(f32[1024,1024,2]{1,0,2:T(8,128)} %get-tuple-element.178, f32[1024,2]{0,1:T(2,128)S(1)} %bitcast.127, f32[1024,1,2,128]{0,3,2,1:T(8,128)S(1)} %get-tuple-element.192, f32[1024,2]{0,1:T(2,128)S(1)} %get-tuple-element.179, pred[]{:T(512)S(6)} %compare.14, ...), kind=kOutput, calls=%fused_computation.10.clone.1 | convolution fusion | flops 543948800 | bytes 10764801 | tf_op jit(solution)/shard_map/while/body/eval_jaxpr/tkgr,rkd->tkgd/dot_general | solution.py:61
  210.8 5.4 %bitcast_reduce_fusion.2 = (f32[1024,2]{0,1:T(2,128)S(1)}, f32[1024,1024,2]{1,0,2:T(8,128)}) fusion(bf16[1024,1,2,128]{3,0,2,1:T(8,128)(2,1)S(1)} %get-tuple-element.203, bf16[16,1024,128]{2,1,0:T(8,128)(2,1)} %get-tuple-element.202, s32[]{:T(128)} %get-tuple-element.189), kind=kOutput, calls=%fused_computation.1.clone.1 | convolution fusion | flops 541063168 | bytes 9183744 | tf_op jit(solution)/shard_map/while/body/eval_jaxpr/tkgd,rkd->tkgr/dot_general | solution.py:54
  216.2 5.5 %fusion.61 = f32[1024,1,2,128]{0,3,2,1:T(8,128)S(1)} fusion(f32[1024,1024,2]{1,0,2:T(8,128)} %get-tuple-element.178, f32[1024,2]{0,1:T(2,128)S(1)} %bitcast.127, f32[1024,1,2,128]{0,3,2,1:T(8,128)S(1)} %get-tuple-element.192, f32[1024,2]{0,1:T(2,128)S(1)} %get-tuple-element.179, pred[]{:T(512)S(6)} %compare.14, ...), kind=kOutput, calls=%fused_computation.10.clone.1 | convolution fusion | flops 543948800 | bytes 10764801 | tf_op jit(solution)/shard_map/while/body/eval_jaxpr/tkgr,rkd->tkgd/dot_general | solution.py:61
  223.5 5.4 %bitcast_reduce_fusion.2 = (f32[1024,2]{0,1:T(2,128)S(1)}, f32[1024,1024,2]{1,0,2:T(8,128)}) fusion(bf16[1024,1,2,128]{3,0,2,1:T(8,128)(2,1)S(1)} %get-tuple-element.203, bf16[16,1024,128]{2,1,0:T(8,128)(2,1)} %get-tuple-element.202, s32[]{:T(128)} %get-tuple-element.189), kind=kOutput, calls=%fused_computation.1.clone.1 | convolution fusion | flops 541063168 | bytes 9183744 | tf_op jit(solution)/shard_map/while/body/eval_jaxpr/tkgd,rkd->tkgr/dot_general | solution.py:54
  229.0 5.5 %fusion.61 = f32[1024,1,2,128]{0,3,2,1:T(8,128)S(1)} fusion(f32[1024,1024,2]{1,0,2:T(8,128)} %get-tuple-element.178, f32[1024,2]{0,1:T(2,128)S(1)} %bitcast.127, f32[1024,1,2,128]{0,3,2,1:T(8,128)S(1)} %get-tuple-element.192, f32[1024,2]{0,1:T(2,128)S(1)} %get-tuple-element.179, pred[]{:T(512)S(6)} %compare.14, ...), kind=kOutput, calls=%fused_computation.10.clone.1 | convolution fusion | flops 543948800 | bytes 10764801 | tf_op jit(solution)/shard_map/while/body/eval_jaxpr/tkgr,rkd->tkgd/dot_general | solution.py:61
  241.7 5.5 %fusion.61 = f32[1024,1,2,128]{0,3,2,1:T(8,128)S(1)} fusion(f32[1024,1024,2]{1,0,2:T(8,128)} %get-tuple-element.178, f32[1024,2]{0,1:T(2,128)S(1)} %bitcast.127, f32[1024,1,2,128]{0,3,2,1:T(8,128)S(1)} %get-tuple-element.192, f32[1024,2]{0,1:T(2,128)S(1)} %get-tuple-element.179, pred[]{:T(512)S(6)} %compare.14, ...), kind=kOutput, calls=%fused_computation.10.clone.1 | convolution fusion | flops 543948800 | bytes 10764801 | tf_op jit(solution)/shard_map/while/body/eval_jaxpr/tkgr,rkd->tkgd/dot_general | solution.py:61
  249.0 5.4 %bitcast_reduce_fusion.2 = (f32[1024,2]{0,1:T(2,128)S(1)}, f32[1024,1024,2]{1,0,2:T(8,128)}) fusion(bf16[1024,1,2,128]{3,0,2,1:T(8,128)(2,1)S(1)} %get-tuple-element.203, bf16[16,1024,128]{2,1,0:T(8,128)(2,1)} %get-tuple-element.202, s32[]{:T(128)} %get-tuple-element.189), kind=kOutput, calls=%fused_computation.1.clone.1 | convolution fusion | flops 541063168 | bytes 9183744 | tf_op jit(solution)/shard_map/while/body/eval_jaxpr/tkgd,rkd->tkgr/dot_general | solution.py:54
  254.4 5.5 %fusion.61 = f32[1024,1,2,128]{0,3,2,1:T(8,128)S(1)} fusion(f32[1024,1024,2]{1,0,2:T(8,128)} %get-tuple-element.178, f32[1024,2]{0,1:T(2,128)S(1)} %bitcast.127, f32[1024,1,2,128]{0,3,2,1:T(8,128)S(1)} %get-tuple-element.192, f32[1024,2]{0,1:T(2,128)S(1)} %get-tuple-element.179, pred[]{:T(512)S(6)} %compare.14, ...), kind=kOutput, calls=%fused_computation.10.clone.1 | convolution fusion | flops 543948800 | bytes 10764801 | tf_op jit(solution)/shard_map/while/body/eval_jaxpr/tkgr,rkd->tkgd/dot_general | solution.py:61
  261.7 5.4 %bitcast_reduce_fusion.2 = (f32[1024,2]{0,1:T(2,128)S(1)}, f32[1024,1024,2]{1,0,2:T(8,128)}) fusion(bf16[1024,1,2,128]{3,0,2,1:T(8,128)(2,1)S(1)} %get-tuple-element.203, bf16[16,1024,128]{2,1,0:T(8,128)(2,1)} %get-tuple-element.202, s32[]{:T(128)} %get-tuple-element.189), kind=kOutput, calls=%fused_computation.1.clone.1 | convolution fusion | flops 541063168 | bytes 9183744 | tf_op jit(solution)/shard_map/while/body/eval_jaxpr/tkgd,rkd->tkgr/dot_general | solution.py:54
  267.2 5.5 %fusion.61 = f32[1024,1,2,128]{0,3,2,1:T(8,128)S(1)} fusion(f32[1024,1024,2]{1,0,2:T(8,128)} %get-tuple-element.178, f32[1024,2]{0,1:T(2,128)S(1)} %bitcast.127, f32[1024,1,2,128]{0,3,2,1:T(8,128)S(1)} %get-tuple-element.192, f32[1024,2]{0,1:T(2,128)S(1)} %get-tuple-element.179, pred[]{:T(512)S(6)} %compare.14, ...), kind=kOutput, calls=%fused_computation.10.clone.1 | convolution fusion | flops 543948800 | bytes 10764801 | tf_op jit(solution)/shard_map/while/body/eval_jaxpr/tkgr,rkd->tkgd/dot_general | solution.py:61
  279.9 5.5 %fusion.61 = f32[1024,1,2,128]{0,3,2,1:T(8,128)S(1)} fusion(f32[1024,1024,2]{1,0,2:T(8,128)} %get-tuple-element.178, f32[1024,2]{0,1:T(2,128)S(1)} %bitcast.127, f32[1024,1,2,128]{0,3,2,1:T(8,128)S(1)} %get-tuple-element.192, f32[1024,2]{0,1:T(2,128)S(1)} %get-tuple-element.179, pred[]{:T(512)S(6)} %compare.14, ...), kind=kOutput, calls=%fused_computation.10.clone.1 | convolution fusion | flops 543948800 | bytes 10764801 | tf_op jit(solution)/shard_map/while/body/eval_jaxpr/tkgr,rkd->tkgd/dot_general | solution.py:61
  287.2 5.4 %bitcast_reduce_fusion.2 = (f32[1024,2]{0,1:T(2,128)S(1)}, f32[1024,1024,2]{1,0,2:T(8,128)}) fusion(bf16[1024,1,2,128]{3,0,2,1:T(8,128)(2,1)S(1)} %get-tuple-element.203, bf16[16,1024,128]{2,1,0:T(8,128)(2,1)} %get-tuple-element.202, s32[]{:T(128)} %get-tuple-element.189), kind=kOutput, calls=%fused_computation.1.clone.1 | convolution fusion | flops 541063168 | bytes 9183744 | tf_op jit(solution)/shard_map/while/body/eval_jaxpr/tkgd,rkd->tkgr/dot_general | solution.py:54
  292.6 5.5 %fusion.61 = f32[1024,1,2,128]{0,3,2,1:T(8,128)S(1)} fusion(f32[1024,1024,2]{1,0,2:T(8,128)} %get-tuple-element.178, f32[1024,2]{0,1:T(2,128)S(1)} %bitcast.127, f32[1024,1,2,128]{0,3,2,1:T(8,128)S(1)} %get-tuple-element.192, f32[1024,2]{0,1:T(2,128)S(1)} %get-tuple-element.179, pred[]{:T(512)S(6)} %compare.14, ...), kind=kOutput, calls=%fused_computation.10.clone.1 | convolution fusion | flops 543948800 | bytes 10764801 | tf_op jit(solution)/shard_map/while/body/eval_jaxpr/tkgr,rkd->tkgd/dot_general | solution.py:61
  300.2 14.4 %all_to_all.24 = bf16[8,128,256]{1,2,0:T(8,128)(2,1)S(1)} all-to-all(bf16[8,128,256]{1,2,0:T(8,128)(2,1)S(1)} %copy.31), channel_id=1, replica_groups=mesh['sp'=16,'tp'=8] {'tp'}, dimensions={0} | all-to-all | bytes 1048576 | tf_op jit(solution)/shard_map/all_to_all | solution.py:107
  326.9 49.4 %all-to-all-done.1 = bf16[8,128,2048]{2,1,0:T(8,128)(2,1)} async-done(((bf16[8,128,2048]{2,1,0:T(8,128)(2,1)}), bf16[8,128,2048]{2,1,0:T(8,128)(2,1)}, u32[]{:S(2)}, u32[]{:S(2)}) %all-to-all-start.1) | async-done | bytes 4194336 | tf_op jit(solution)/shard_map/all_to_all | solution.py:114
  376.3 14.4 %convolution_convert_fusion = bf16[1024,2048]{1,0:T(8,128)(2,1)} fusion(bf16[1024,2048]{1,0:T(8,128)(2,1)} %all-gather.8.cloned.1.call-done, bf16[1024,2048]{1,0:T(8,128)(2,1)} %bitcast.16, bf16[2048,1024]{1,0:T(8,128)(2,1)} %all-gather.6.cloned.1.call-done), kind=kOutput, calls=%fused_computation.28 | convolution fusion | flops 8595177472 | bytes 16777216 | tf_op jit(solution)/shard_map/dot_general | solution.py:126
  390.7 36.3 %reduce-scatter.2.cloned.1.call-done = bf16[128,2048]{1,0:T(8,128)(2,1)} async-done(((bf16[1024,2048]{1,0:T(8,128)(2,1)}), bf16[128,2048]{1,0:T(8,128)(2,1)}) %reduce-scatter.2.cloned.1.call-update) | async-done | bytes 524304 | tf_op jit(solution)/shard_map/reduce_scatter | solution.py:125
  (157 shorter events, 96.9 us)
Async XLA Ops:
  6.5 4.4 %copy-start.1 = (bf16[1024,128]{1,0:T(8,128)(2,1)S(1)}, bf16[1024,128]{1,0:T(8,128)(2,1)}, u32[]{:S(2)}) copy-start(bf16[1024,128]{1,0:T(8,128)(2,1)} %param.14) | copy-start | bytes 786436
  6.5 4.4 %copy-start.5 = (f32[128]{0:T(128)S(1)}, f32[128]{0:T(128)}, u32[]{:S(2)}) copy-start(f32[128]{0:T(128)} %param.17) | copy-start | bytes 1540
  6.5 82.9 %all-gather.4.cloned.1.call-start = ((), (), s32[]{:S(2)}) async-start(), calls=%async_computation.3 | async-start | bytes 8912896 | tf_op jit(solution)/shard_map/all_gather | solution.py:14
  8.9 6.1 %copy-start.3 = (bf16[1024,128]{1,0:T(8,128)(2,1)S(1)}, bf16[1024,128]{1,0:T(8,128)(2,1)}, u32[]{:S(2)}) copy-start(bf16[1024,128]{1,0:T(8,128)(2,1)} %param.15) | copy-start | bytes 786436
  10.9 8.1 %copy-start.6 = (f32[128]{0:T(128)S(1)}, f32[128]{0:T(128)}, u32[]{:S(2)}) copy-start(f32[128]{0:T(128)} %param.16) | copy-start | bytes 1540
  15.9 311.0 %all-gather.6.cloned.1.call-start = ((), (), s32[]{:S(2)}) async-start(), calls=%async_computation.4 | async-start | bytes 4456448 | tf_op jit(solution)/shard_map/all_gather | solution.py:119
  16.6 310.3 %all-gather.8.cloned.1.call-start = ((), (), s32[]{:S(2)}) async-start(), calls=%async_computation.5 | async-start | bytes 4456448 | tf_op jit(solution)/shard_map/all_gather | solution.py:124
  100.6 6.0 %copy-start = (f32[1024,1024,2]{1,0,2:T(8,128)S(1)}, f32[1024,1024,2]{1,0,2:T(8,128)}, u32[]{:S(2)}) copy-start(f32[1024,1024,2]{1,0,2:T(8,128)} %get-tuple-element.178) | copy-start | bytes 25165828 | tf_op jit(solution)/shard_map/while
  113.5 5.8 %copy-start = (f32[1024,1024,2]{1,0,2:T(8,128)S(1)}, f32[1024,1024,2]{1,0,2:T(8,128)}, u32[]{:S(2)}) copy-start(f32[1024,1024,2]{1,0,2:T(8,128)} %get-tuple-element.178) | copy-start | bytes 25165828 | tf_op jit(solution)/shard_map/while
  126.2 6.1 %copy-start = (f32[1024,1024,2]{1,0,2:T(8,128)S(1)}, f32[1024,1024,2]{1,0,2:T(8,128)}, u32[]{:S(2)}) copy-start(f32[1024,1024,2]{1,0,2:T(8,128)} %get-tuple-element.178) | copy-start | bytes 25165828 | tf_op jit(solution)/shard_map/while
  139.2 5.8 %copy-start = (f32[1024,1024,2]{1,0,2:T(8,128)S(1)}, f32[1024,1024,2]{1,0,2:T(8,128)}, u32[]{:S(2)}) copy-start(f32[1024,1024,2]{1,0,2:T(8,128)} %get-tuple-element.178) | copy-start | bytes 25165828 | tf_op jit(solution)/shard_map/while
  152.0 6.1 %copy-start = (f32[1024,1024,2]{1,0,2:T(8,128)S(1)}, f32[1024,1024,2]{1,0,2:T(8,128)}, u32[]{:S(2)}) copy-start(f32[1024,1024,2]{1,0,2:T(8,128)} %get-tuple-element.178) | copy-start | bytes 25165828 | tf_op jit(solution)/shard_map/while
  165.0 5.9 %copy-start = (f32[1024,1024,2]{1,0,2:T(8,128)S(1)}, f32[1024,1024,2]{1,0,2:T(8,128)}, u32[]{:S(2)}) copy-start(f32[1024,1024,2]{1,0,2:T(8,128)} %get-tuple-element.178) | copy-start | bytes 25165828 | tf_op jit(solution)/shard_map/while
  177.7 5.9 %copy-start = (f32[1024,1024,2]{1,0,2:T(8,128)S(1)}, f32[1024,1024,2]{1,0,2:T(8,128)}, u32[]{:S(2)}) copy-start(f32[1024,1024,2]{1,0,2:T(8,128)} %get-tuple-element.178) | copy-start | bytes 25165828 | tf_op jit(solution)/shard_map/while
  190.5 6.1 %copy-start = (f32[1024,1024,2]{1,0,2:T(8,128)S(1)}, f32[1024,1024,2]{1,0,2:T(8,128)}, u32[]{:S(2)}) copy-start(f32[1024,1024,2]{1,0,2:T(8,128)} %get-tuple-element.178) | copy-start | bytes 25165828 | tf_op jit(solution)/shard_map/while
  203.5 5.8 %copy-start = (f32[1024,1024,2]{1,0,2:T(8,128)S(1)}, f32[1024,1024,2]{1,0,2:T(8,128)}, u32[]{:S(2)}) copy-start(f32[1024,1024,2]{1,0,2:T(8,128)} %get-tuple-element.178) | copy-start | bytes 25165828 | tf_op jit(solution)/shard_map/while
  216.2 5.8 %copy-start = (f32[1024,1024,2]{1,0,2:T(8,128)S(1)}, f32[1024,1024,2]{1,0,2:T(8,128)}, u32[]{:S(2)}) copy-start(f32[1024,1024,2]{1,0,2:T(8,128)} %get-tuple-element.178) | copy-start | bytes 25165828 | tf_op jit(solution)/shard_map/while
  229.0 5.8 %copy-start = (f32[1024,1024,2]{1,0,2:T(8,128)S(1)}, f32[1024,1024,2]{1,0,2:T(8,128)}, u32[]{:S(2)}) copy-start(f32[1024,1024,2]{1,0,2:T(8,128)} %get-tuple-element.178) | copy-start | bytes 25165828 | tf_op jit(solution)/shard_map/while
  241.7 5.8 %copy-start = (f32[1024,1024,2]{1,0,2:T(8,128)S(1)}, f32[1024,1024,2]{1,0,2:T(8,128)}, u32[]{:S(2)}) copy-start(f32[1024,1024,2]{1,0,2:T(8,128)} %get-tuple-element.178) | copy-start | bytes 25165828 | tf_op jit(solution)/shard_map/while
  254.4 5.8 %copy-start = (f32[1024,1024,2]{1,0,2:T(8,128)S(1)}, f32[1024,1024,2]{1,0,2:T(8,128)}, u32[]{:S(2)}) copy-start(f32[1024,1024,2]{1,0,2:T(8,128)} %get-tuple-element.178) | copy-start | bytes 25165828 | tf_op jit(solution)/shard_map/while
  267.1 5.8 %copy-start = (f32[1024,1024,2]{1,0,2:T(8,128)S(1)}, f32[1024,1024,2]{1,0,2:T(8,128)}, u32[]{:S(2)}) copy-start(f32[1024,1024,2]{1,0,2:T(8,128)} %get-tuple-element.178) | copy-start | bytes 25165828 | tf_op jit(solution)/shard_map/while
  279.9 5.8 %copy-start = (f32[1024,1024,2]{1,0,2:T(8,128)S(1)}, f32[1024,1024,2]{1,0,2:T(8,128)}, u32[]{:S(2)}) copy-start(f32[1024,1024,2]{1,0,2:T(8,128)} %get-tuple-element.178) | copy-start | bytes 25165828 | tf_op jit(solution)/shard_map/while
  292.6 5.8 %copy-start = (f32[1024,1024,2]{1,0,2:T(8,128)S(1)}, f32[1024,1024,2]{1,0,2:T(8,128)}, u32[]{:S(2)}) copy-start(f32[1024,1024,2]{1,0,2:T(8,128)} %get-tuple-element.178) | copy-start | bytes 25165828 | tf_op jit(solution)/shard_map/while
  299.9 14.8 %copy-start.2 = (bf16[128,2048]{1,0:T(8,128)(2,1)S(1)}, bf16[128,2048]{1,0:T(8,128)(2,1)}, u32[]{:S(2)}) copy-start(bf16[128,2048]{1,0:T(8,128)(2,1)} %param.12) | copy-start | bytes 1572868
  314.6 4.8 %copy-start.4 = (f32[2048]{0:T(1024)S(1)}, f32[2048]{0:T(1024)}, u32[]{:S(2)}) copy-start(f32[2048]{0:T(1024)} %param.19) | copy-start | bytes 24580
  322.1 54.2 %all-to-all-start.1 = ((bf16[8,128,2048]{2,1,0:T(8,128)(2,1)}), bf16[8,128,2048]{2,1,0:T(8,128)(2,1)}, u32[]{:S(2)}, u32[]{:S(2)}) async-start(bf16[8,128,2048]{2,1,0:T(8,128)(2,1)} %stack.2), calls=%async_computation.1 | async-start | bytes 8388608 | tf_op jit(solution)/shard_map/all_to_all | solution.py:114
  326.6 100.3 %reduce-scatter.2.cloned.1.call-start = ((), (), s32[]{:S(2)}) async-start(), calls=%async_computation.6 | async-start | bytes 4718592 | tf_op jit(solution)/shard_map/reduce_scatter | solution.py:125
Sparse Core Ops, SparseCore 0:
  16.0 73.4 all-gather.3
  91.6 51.0 all-gather.5
  144.8 56.5 all-gather.7
  390.8 36.0 reduce-scatter.1
